TPU v7x, 32 devices: a whole 2x2x4 slice. The times are simulated.
32 devices in a mesh: sp: 8 (over z, y), tp: 4 (over x, core).
Axes of the slice: x: 2, y: 2, z: 4, core: 2. Of those that a mesh axis runs over, the one named last changes fastest.
Arguments:
- tokens: bfloat16 [2560, 2048], P('sp', 'tp'), may hold values from -6 to 6
- pre_gain: float32 [2, 2048], replicated, may hold values from 0.1 to 1.9
- w_value: bfloat16 [2, 2048, 2048], P(None, 'sp', 'tp'), may hold values from -0.125 to 0.125
- w_gate: bfloat16 [2, 2048, 2048], P(None, 'sp', 'tp'), may hold values from -0.125 to 0.125
- taps: float32 [2, 31, 2048], P(None, None, 'tp'), may hold values from -5 to 5
- norm_gain: float32 [2, 2048], P(None, 'tp'), may hold values from 0.1 to 1.9
- norm_shift: float32 [2, 2048], P(None, 'tp'), may hold values from -3 to 3
- w_out: bfloat16 [2, 2048, 2048], P(None, 'tp', 'sp'), may hold values from -2 to 2
- post_gain: float32 [2, 2048], P(None, 'tp'), may hold values from 0.1 to 1.9
Outputs:
- stream: bfloat16 [2560, 2048], P('sp', 'tp')
All inputs are finite; a program needn't handle non-finite values.
Results may differ from a plain program's by a relative error of at most 0.015.
Values may be sent and summed in bfloat16 or wider, within the bound.
A program may use at most 64 MiB of HBM per device.

v0:
```python
import jax
import jax.numpy as jnp
from jax import lax
from jax.sharding import PartitionSpec as P

D = 2048
CONV_WIDTH = 31
LAYERS = 2
EPSILON = 1e-06
LN_EPSILON = 1e-05


def passed_along(block, axis, distance):
    devices = range(lax.axis_size(axis))
    route = [(i - distance, i) for i in devices if i - distance in devices]
    return lax.ppermute(block, axis, route)


def local(tokens, pre_gain, w_value, w_gate, taps, norm_gain, norm_shift, w_out, post_gain):
    stream = tokens
    full_value, full_gate = (
        lax.all_gather(w_value, "sp", axis=1, tiled=True),
        lax.all_gather(w_gate, "sp", axis=1, tiled=True),
    )
    full_out = lax.all_gather(w_out, "sp", axis=2, tiled=True)
    for layer in range(LAYERS):
        whole = lax.all_gather(stream, "tp", axis=1, tiled=True)
        whole_f = whole.astype(jnp.float32)
        normed = (
            whole_f
            * lax.rsqrt(jnp.mean(whole_f * whole_f, -1, keepdims=True) + EPSILON)
            * pre_gain[layer]
        ).astype(jnp.bfloat16)
        value_mat = full_value[layer]
        gate_mat = full_gate[layer]
        out_mat = full_out[layer]
        value_proj = jnp.dot(normed, value_mat, preferred_element_type=jnp.float32)
        gate_proj = jnp.dot(normed, gate_mat, preferred_element_type=jnp.float32)
        glu_act = (value_proj * jax.nn.sigmoid(gate_proj)).astype(jnp.bfloat16)
        rows = glu_act.shape[0]
        fringe = passed_along(glu_act[rows - (CONV_WIDTH - 1) :], "sp", 1)
        padded = jnp.concatenate([fringe, glu_act], 0).astype(jnp.float32)
        conv_out = jnp.zeros(glu_act.shape, jnp.float32)
        for offset in range(CONV_WIDTH):
            conv_out = conv_out + taps[layer, offset] * padded[offset : offset + rows]
        row_sum, row_square = lax.psum(
            (jnp.sum(conv_out, -1, keepdims=True), jnp.sum(conv_out * conv_out, -1, keepdims=True)),
            "tp",
        )
        center = row_sum / D
        spread = jnp.maximum(row_square / D - center * center, 0.0)
        activated = jax.nn.silu(
            (conv_out - center) * lax.rsqrt(spread + LN_EPSILON) * norm_gain[layer]
            + norm_shift[layer]
        ).astype(jnp.bfloat16)
        terms = jnp.dot(activated, out_mat, preferred_element_type=jnp.float32)
        summed = lax.psum_scatter(terms.astype(jnp.bfloat16), "tp", scatter_dimension=1, tiled=True)
        projected = summed.astype(jnp.float32)
        out_square = lax.psum(jnp.sum(projected * projected, -1, keepdims=True), "tp")
        scale = lax.rsqrt(out_square / D + EPSILON)
        stream = (stream.astype(jnp.float32) + projected * scale * post_gain[layer]).astype(
            jnp.bfloat16
        )
    return stream


def solution(mesh):
    placed = (
        P("sp", "tp"),
        P(),
        P(None, "sp", "tp"),
        P(None, "sp", "tp"),
        P(None, None, "tp"),
        P(None, "tp"),
        P(None, "tp"),
        P(None, "tp", "sp"),
        P(None, "tp"),
    )
    return jax.shard_map(
        local, mesh=mesh, in_specs=placed, out_specs=P("sp", "tp"), check_vma=False
    )
```

profile of v0, /device:TPU:0, one launch (start us, length us, event | category | flops | bytes accessed | tf_op | source)
XLA Modules:
  0.0 377.1 jit_solution(16301794310421925368)
XLA Ops:
  6.5 0.7 all-gather.6.cloned.1.call-update
  7.3 0.0 all-gather.10.cloned.1.call-start
  7.3 0.7 all-gather.10.cloned.1.call-update
  8.0 0.0 all-gather.8.cloned.1.call-start
  8.1 0.7 all-gather.8.cloned.1.call-update
  8.7 0.0 all-gather.12.cloned.1.call-start
  8.8 0.5 all-gather.12.cloned.1.call-update
  9.3 0.0 reduce-scatter.3.cloned.1.call-start
  9.4 0.8 fusion.116
  10.1 0.8 fusion.113
  10.9 0.9 fusion.112
  11.8 0.9 fusion.111
  12.7 0.8 fusion.114
  13.5 16.3 %all-gather.6.cloned.1.call-done = bf16[320,2048]{1,0:T(8,128)(2,1)} async-done(((bf16[320,512]{1,0:T(8,128)(2,1)}), bf16[320,2048]{1,0:T(8,128)(2,1)}) %all-gather.6.cloned.1.call-update) | async-done | bytes 1310736 | tf_op jit(solution)/shard_map/all_gather | solution.py:27
  29.8 1.7 fusion
  31.5 73.3 %all-gather.10.cloned.1.call-done = bf16[2,2048,512]{2,1,0:T(8,128)(2,1)} async-done(((bf16[2,256,512]{2,1,0:T(8,128)(2,1)}), bf16[2,2048,512]{2,1,0:T(8,128)(2,1)}) %all-gather.10.cloned.1.call-update) | async-done | bytes 4194320 | tf_op jit(solution)/shard_map/all_gather | solution.py:23
  104.8 3.1 fusion.20
  107.9 70.4 %all-gather.8.cloned.1.call-done = bf16[2,2048,512]{2,1,0:T(8,128)(2,1)} async-done(((bf16[2,256,512]{2,1,0:T(8,128)(2,1)}), bf16[2,2048,512]{2,1,0:T(8,128)(2,1)}) %all-gather.8.cloned.1.call-update) | async-done | bytes 4194320 | tf_op jit(solution)/shard_map/all_gather | solution.py:22
  178.3 2.5 fusion.19
  180.8 2.5 collective-permute-start
  183.3 1.6 collective-permute-done
  184.9 0.1 maximum_convert_fusion
  185.0 3.2 fusion.107
  188.2 6.1 %all-reduce.1 = (f32[320,1]{0,1:T(1,128)S(1)}, f32[320,1]{0,1:T(1,128)S(1)}) all-reduce(f32[320,1]{0,1:T(1,128)S(1)} %broadcast_in_dim.20, f32[320,1]{0,1:T(1,128)S(1)} %broadcast_in_dim.21), channel_id=1, replica_groups=mesh['sp'=8,'tp'=4] {'tp'}, use_global_device_ids=true, to_apply=%region_2.0 | all-reduce | flops 640 | bytes 5120 | tf_op jit(solution)/shard_map/psum | solution.py:46
  194.3 59.2 %all-gather.12.cloned.1.call-done = bf16[2,512,2048]{2,1,0:T(8,128)(2,1)} async-done(((bf16[2,512,256]{2,1,0:T(8,128)(2,1)}), bf16[2,512,2048]{2,1,0:T(8,128)(2,1)}) %all-gather.12.cloned.1.call-update) | async-done | bytes 4194320 | tf_op jit(solution)/shard_map/all_gather | solution.py:25
  253.5 3.8 %convolution_convert_fusion.1 = bf16[320,2048]{1,0:T(8,128)(2,1)} fusion(bf16[2,512,2048]{2,1,0:T(8,128)(2,1)} %all-gather.12.cloned.1.call-done, f32[320,512]{1,0:T(8,128)S(1)} %get-tuple-element.18, f32[512]{0:T(512)S(1)} %bitcast.183, f32[512]{0:T(512)S(1)} %bitcast.182, f32[320]{0:T(512)S(1)} %get-tuple-element.12, f32[320]{0:T(512)S(1)} %get-tuple-element.11), kind=kOutput, calls=%fused_computation.5 | convolution fusion | flops 673218560 | bytes 4069888 | tf_op jit(solution)/shard_map/dot_general | solution.py:56
  257.3 0.0 all-gather.14.cloned.1.call-start
  257.3 24.7 %reduce-scatter.3.cloned.1.call-done = bf16[320,512]{1,0:T(8,128)(2,1)} async-done(((bf16[320,2048]{1,0:T(8,128)(2,1)}), bf16[320,512]{1,0:T(8,128)(2,1)}) %reduce-scatter.3.cloned.1.call-update) | async-done | bytes 327696 | tf_op jit(solution)/shard_map/reduce_scatter | solution.py:57
  282.0 1.1 fusion.22
  283.2 5.8 %psum.44 = f32[320,1]{0,1:T(1,128)S(1)} all-reduce(f32[320,1]{0,1:T(1,128)S(1)} %broadcast_in_dim.22), channel_id=1, replica_groups=mesh['sp'=8,'tp'=4] {'tp'}, use_global_device_ids=true, to_apply=%region_7.8 | all-reduce | flops 320 | bytes 2560 | tf_op jit(solution)/shard_map/psum | solution.py:59
  289.0 1.9 fusion.25
  290.9 0.0 reduce-scatter.5.cloned.1.call-start
  290.9 18.9 %all-gather.14.cloned.1.call-done = bf16[320,2048]{1,0:T(8,128)(2,1)} async-done(((bf16[320,512]{1,0:T(8,128)(2,1)}), bf16[320,2048]{1,0:T(8,128)(2,1)}) %all-gather.14.cloned.1.call-update) | async-done | bytes 1310736 | tf_op jit(solution)/shard_map/all_gather | solution.py:27
  309.8 1.7 fusion.3
  311.5 3.1 fusion.21
  314.6 0.5 copy-done.6
  315.1 0.9 fusion.18
  316.0 3.4 collective-permute-start.1
  319.4 0.9 fusion.110
  320.3 0.7 collective-permute-done.1
  321.0 0.1 maximum_convert_fusion.1
  321.1 3.2 fusion.106
  324.3 6.0 %all-reduce = (f32[320,1]{0,1:T(1,128)S(1)}, f32[320,1]{0,1:T(1,128)S(1)}) all-reduce(f32[320,1]{0,1:T(1,128)S(1)} %broadcast_in_dim.23, f32[320,1]{0,1:T(1,128)S(1)} %broadcast_in_dim.24), channel_id=1, replica_groups=mesh['sp'=8,'tp'=4] {'tp'}, use_global_device_ids=true, to_apply=%region_10.11 | all-reduce | flops 640 | bytes 5120 | tf_op jit(solution)/shard_map/psum | solution.py:46
  330.3 3.7 convolution_convert_fusion
  334.0 27.4 %reduce-scatter.5.cloned.1.call-done = bf16[320,512]{1,0:T(8,128)(2,1)} async-done(((bf16[320,2048]{1,0:T(8,128)(2,1)}), bf16[320,512]{1,0:T(8,128)(2,1)}) %reduce-scatter.5.cloned.1.call-update) | async-done | bytes 327696 | tf_op jit(solution)/shard_map/reduce_scatter | solution.py:57
  361.4 1.1 fusion.26
  362.5 5.8 %psum.47 = f32[320,1]{0,1:T(1,128)S(1)} all-reduce(f32[320,1]{0,1:T(1,128)S(1)} %broadcast_in_dim.25), channel_id=1, replica_groups=mesh['sp'=8,'tp'=4] {'tp'}, use_global_device_ids=true, to_apply=%region_15.16 | all-reduce | flops 320 | bytes 2560 | tf_op jit(solution)/shard_map/psum | solution.py:59
  368.3 1.9 fusion.29
  (33 shorter events, 0.3 us)
Async XLA Ops:
  6.5 23.3 %all-gather.6.cloned.1.call-start = ((), (), s32[]{:S(2)}) async-start(), calls=%async_computation.2 | async-start | bytes 1638400 | tf_op jit(solution)/shard_map/all_gather | solution.py:27
  7.3 97.5 %all-gather.10.cloned.1.call-start = ((), (), s32[]{:S(2)}) async-start(), calls=%async_computation.4 | async-start | bytes 4718592 | tf_op jit(solution)/shard_map/all_gather | solution.py:23
  8.0 170.3 %all-gather.8.cloned.1.call-start = ((), (), s32[]{:S(2)}) async-start(), calls=%async_computation.3 | async-start | bytes 4718592 | tf_op jit(solution)/shard_map/all_gather | solution.py:22
  8.7 244.7 %all-gather.12.cloned.1.call-start = ((), (), s32[]{:S(2)}) async-start(), calls=%async_computation.5 | async-start | bytes 4718592 | tf_op jit(solution)/shard_map/all_gather | solution.py:25
  9.3 272.7 %reduce-scatter.3.cloned.1.call-start = ((), (), s32[]{:S(2)}) async-start(), calls=%async_computation.6 | async-start | bytes 1638400 | tf_op jit(solution)/shard_map/reduce_scatter | solution.py:57
  104.8 73.5 %copy-start.1 = (bf16[320,2048]{1,0:T(8,128)(2,1)S(1)}, bf16[320,2048]{1,0:T(8,128)(2,1)}, u32[]{:S(2)}) copy-start(bf16[320,2048]{1,0:T(8,128)(2,1)} %all-gather.6.cloned.1.call-done) | copy-start | bytes 3932164
  107.9 75.4 %copy-start.4 = (f32[2,512]{1,0:T(2,128)S(1)}, f32[2,512]{1,0:T(2,128)}, u32[]{:S(2)}) copy-start(f32[2,512]{1,0:T(2,128)} %param.15) | copy-start | bytes 12292
  180.8 4.0 %collective-permute-start = (bf16[30,512]{1,0:T(8,128)(2,1)S(1)}, bf16[30,512]{1,0:T(8,128)(2,1)S(1)}, u32[]{:S(2)}, u32[]{:S(2)}) collective-permute-start(bf16[30,512]{1,0:T(8,128)(2,1)S(1)} %slice.562), channel_id=1, source_target_pairs={{0,4},{4,8},{8,12},{12,16},{16,20},{20,24},{24,28},{1,5},{5,9},{9,... | collective-permute-start | bytes 92168 | tf_op jit(solution)/shard_map/ppermute | solution.py:16
  253.4 3.9 %copy-start.5 = (f32[2,512]{1,0:T(2,128)S(1)}, f32[2,512]{1,0:T(2,128)}, u32[]{:S(2)}) copy-start(f32[2,512]{1,0:T(2,128)} %param.17) | copy-start | bytes 12292
  253.4 35.5 %copy-start.3 = (bf16[320,512]{1,0:T(8,128)(2,1)S(1)}, bf16[320,512]{1,0:T(8,128)(2,1)}, u32[]{:S(2)}) copy-start(bf16[320,512]{1,0:T(8,128)(2,1)} %param.9) | copy-start | bytes 983044
  257.3 52.5 %all-gather.14.cloned.1.call-start = ((), (), s32[]{:S(2)}) async-start(), calls=%async_computation.7 | async-start | bytes 1638400 | tf_op jit(solution)/shard_map/all_gather | solution.py:27
  290.9 70.5 %reduce-scatter.5.cloned.1.call-start = ((), (), s32[]{:S(2)}) async-start(), calls=%async_computation.8 | async-start | bytes 1638400 | tf_op jit(solution)/shard_map/reduce_scatter | solution.py:57
  311.5 3.1 copy-start.2
  311.5 3.6 copy-start.6
  316.0 5.0 %collective-permute-start.1 = (bf16[30,512]{1,0:T(8,128)(2,1)S(1)}, bf16[30,512]{1,0:T(8,128)(2,1)S(1)}, u32[]{:S(2)}, u32[]{:S(2)}) collective-permute-start(bf16[30,512]{1,0:T(8,128)(2,1)S(1)} %slice.597), channel_id=1, source_target_pairs={{0,4},{4,8},{8,12},{12,16},{16,20},{20,24},{24,28},{1,5},{5,9},{9,... | collective-permute-start | bytes 92168 | tf_op jit(solution)/shard_map/ppermute | solution.py:16
  330.3 38.1 %copy-start = (bf16[320,512]{1,0:T(8,128)(2,1)S(1)}, bf16[320,512]{1,0:T(8,128)(2,1)}, u32[]{:S(2)}) copy-start(bf16[320,512]{1,0:T(8,128)(2,1)} %fusion.25) | copy-start | bytes 983044
Sparse Core Ops, SparseCore 0:
  8.9 20.8 all-gather.5
  32.0 72.7 all-gather.9
  107.0 71.2 all-gather.7
  180.2 73.1 all-gather.11
  257.4 24.5 reduce-scatter.2
  291.0 18.7 all-gather.13
  334.1 27.2 reduce-scatter.4
where the time goes:
time: 378 us; the launch traced here: 377 us
  waiting for transfers between devices  295 us (78%)
  blocking collectives  23.5 us (6%)
  matrix products  17 us (4%)
  other arithmetic  16 us (4%)
  between operations  13.7 us (4%)
  starting transfers between devices  6.07 us (2%)
  local copies, waits for them, and re-layouts  5.61 us (1%)
    all_gather x1, waiting for transfers between devices, local(): lax.all_gather(w_gate, 'sp', axis=1, tiled=True)  73.3 us
    all_gather x1, waiting for transfers between devices, local(): lax.all_gather(w_value, 'sp', axis=1, tiled=True)  70.4 us
    all_gather x1, waiting for transfers between devices, local(): full_out = lax.all_gather(w_out, 'sp', axis=2, tiled=True)  59.2 us
    reduce_scatter x2, waiting for transfers between devices, local(): lax.psum_scatter(terms.astype(jnp.bfloat16), 'tp', scatter_dimension=1, t...  52.1 us
    all_gather x2, waiting for transfers between devices, local(): whole = lax.all_gather(stream, 'tp', axis=1, tiled=True)  35.2 us
    psum x2, blocking collectives, local(): lax.psum((jnp.sum(conv_out, -1, keepdims=True), jnp.sum(conv_out * conv_o...  12 us
    psum x2, blocking collectives, local(): lax.psum(jnp.sum(projected * projected, -1, keepdims=True), 'tp')  11.5 us
  transfers between devices with their start and end apart: 9, of which 9 were waited for; matrix products, arithmetic and copies ran while one was open for 4% of the time, Pallas kernels for 0%

commit v1 on v0

--- a/solution.py
+++ b/solution.py
@@ -22,7 +22,12 @@
         lax.all_gather(w_value, "sp", axis=1, tiled=True),
         lax.all_gather(w_gate, "sp", axis=1, tiled=True),
     )
-    full_out = lax.all_gather(w_out, "sp", axis=2, tiled=True)
+    ring = [w_out]
+    for hop in range(7):
+        ring.append(lax.ppermute(ring[-1], "sp", [(dev, (dev + 1) % 8) for dev in range(8)]))
+    full_out = jnp.roll(
+        jnp.concatenate(ring[::-1], axis=2), (lax.axis_index("sp") + 1) * ring[0].shape[2], axis=2
+    )
     for layer in range(LAYERS):
         whole = lax.all_gather(stream, "tp", axis=1, tiled=True)
         whole_f = whole.astype(jnp.float32)

time: 378 us -> 363 us (0.960)
  waiting for transfers between devices: 295 us -> 258 us
  local copies, waits for them, and re-layouts: 5.61 us -> 24.7 us
    ppermute x0 -> x7, waiting for transfers between devices: none -> 137 us  [local(): lax.ppermute(ring[-1], 'sp', [(dev, (dev + 1) % 8) for dev in range(8)])]
    all_gather x1, waiting for transfers between devices: 73.3 us -> 0.01 us  [local(): lax.all_gather(w_gate, 'sp', axis=1, tiled=True)]
    all_gather x1 -> x0, waiting for transfers between devices: 59.2 us -> none  [local(): full_out = lax.all_gather(w_out, 'sp', axis=2, tiled=True)]
    all_gather x1, waiting for transfers between devices: 70.4 us -> 44 us  [local(): lax.all_gather(w_value, 'sp', axis=1, tiled=True)]
    unnamed x14 -> x29, local copies, waits for them, and re-layouts: 0.5 us -> 18 us
    all_gather x2, waiting for transfers between devices: 35.2 us -> 18.9 us  [local(): whole = lax.all_gather(stream, 'tp', axis=1, tiled=True)]
  transfers between devices with their start and end apart: 9 -> 15, of which waited for: 9 -> 13; matrix products, arithmetic and copies ran while one was open for 4% -> 8% of each run, Pallas kernels for 0% -> 0%
where the time goes in v1:
time: 363 us; the launch traced here: 362 us
  waiting for transfers between devices  258 us (71%)
  local copies, waits for them, and re-layouts  24.7 us (7%)
  blocking collectives  23.3 us (6%)
  matrix products  17.1 us (5%)
  other arithmetic  16.1 us (4%)
  between operations  13.7 us (4%)
  starting transfers between devices  9.09 us (3%)
    ppermute x7, waiting for transfers between devices, local(): lax.ppermute(ring[-1], 'sp', [(dev, (dev + 1) % 8) for dev in range(8)])  137 us
    reduce_scatter x2, waiting for transfers between devices, local(): lax.psum_scatter(terms.astype(jnp.bfloat16), 'tp', scatter_dimension=1, t...  55.4 us
    all_gather x1, waiting for transfers between devices, local(): lax.all_gather(w_value, 'sp', axis=1, tiled=True)  44 us
    all_gather x2, waiting for transfers between devices, local(): whole = lax.all_gather(stream, 'tp', axis=1, tiled=True)  18.9 us
    unnamed x29, local copies, waits for them, and re-layouts  18 us
    psum x2, blocking collectives, local(): lax.psum((jnp.sum(conv_out, -1, keepdims=True), jnp.sum(conv_out * conv_o...  11.7 us
    psum x2, blocking collectives, local(): lax.psum(jnp.sum(projected * projected, -1, keepdims=True), 'tp')  11.5 us
    dot_general x2, matrix products, local(): terms = jnp.dot(activated, out_mat, preferred_element_type=jnp.float32)  7.48 us
  transfers between devices with their start and end apart: 15, of which 13 were waited for; matrix products, arithmetic and copies ran while one was open for 8% of the time, Pallas kernels for 0%

profile of v1, /device:TPU:0, one launch (start us, length us, event | category | flops | bytes accessed | tf_op | source)
XLA Modules:
  0.0 362.2 jit_solution(6028497208586219525)
XLA Ops:
  8.8 3.0 collective-permute-start.1
  11.8 15.2 %collective-permute-done.1 = bf16[2,512,256]{2,1,0:T(8,128)(2,1)S(1)} collective-permute-done((bf16[2,512,256]{2,1,0:T(8,128)(2,1)}, bf16[2,512,256]{2,1,0:T(8,128)(2,1)S(1)}, u32[]{:S(2)}, u32[]{:S(2)}) %collective-permute-start.1) | collective-permute-done | bytes 524320 | tf_op jit(solution)/shard_map/ppermute | solution.py:27
  27.0 15.8 %collective-permute-done.2 = bf16[2,512,256]{2,1,0:T(8,128)(2,1)S(1)} collective-permute-done((bf16[2,512,256]{2,1,0:T(8,128)(2,1)S(1)}, bf16[2,512,256]{2,1,0:T(8,128)(2,1)S(1)}, u32[]{:S(2)}, u32[]{:S(2)}) %collective-permute-start.2) | collective-permute-done | bytes 524320 | tf_op jit(solution)/shard_map/ppermute | solution.py:27
  42.8 27.8 %collective-permute-done.3 = bf16[2,512,256]{2,1,0:T(8,128)(2,1)S(1)} collective-permute-done((bf16[2,512,256]{2,1,0:T(8,128)(2,1)S(1)}, bf16[2,512,256]{2,1,0:T(8,128)(2,1)S(1)}, u32[]{:S(2)}, u32[]{:S(2)}) %collective-permute-start.3) | collective-permute-done | bytes 524320 | tf_op jit(solution)/shard_map/ppermute | solution.py:27
  70.6 21.1 %collective-permute-done.4 = bf16[2,512,256]{2,1,0:T(8,128)(2,1)S(1)} collective-permute-done((bf16[2,512,256]{2,1,0:T(8,128)(2,1)S(1)}, bf16[2,512,256]{2,1,0:T(8,128)(2,1)S(1)}, u32[]{:S(2)}, u32[]{:S(2)}) %collective-permute-start.4) | collective-permute-done | bytes 524320 | tf_op jit(solution)/shard_map/ppermute | solution.py:27
  92.5 0.9 fusion.113
  93.4 0.9 fusion.114
  94.3 24.3 %collective-permute-done.5 = bf16[2,512,256]{2,1,0:T(8,128)(2,1)S(1)} collective-permute-done((bf16[2,512,256]{2,1,0:T(8,128)(2,1)S(1)}, bf16[2,512,256]{2,1,0:T(8,128)(2,1)S(1)}, u32[]{:S(2)}, u32[]{:S(2)}) %collective-permute-start.5) | collective-permute-done | bytes 524320 | tf_op jit(solution)/shard_map/ppermute | solution.py:27
  120.3 22.7 %collective-permute-done.6 = bf16[2,512,256]{2,1,0:T(8,128)(2,1)} collective-permute-done((bf16[2,512,256]{2,1,0:T(8,128)(2,1)S(1)}, bf16[2,512,256]{2,1,0:T(8,128)(2,1)}, u32[]{:S(2)}, u32[]{:S(2)}) %collective-permute-start.6) | collective-permute-done | bytes 524320 | tf_op jit(solution)/shard_map/ppermute | solution.py:27
  143.7 1.7 fusion
  145.5 9.7 %collective-permute-done.7 = bf16[2,512,256]{2,1,0:T(8,128)(2,1)} collective-permute-done((bf16[2,512,256]{2,1,0:T(8,128)(2,1)}, bf16[2,512,256]{2,1,0:T(8,128)(2,1)}, u32[]{:S(2)}, u32[]{:S(2)}) %collective-permute-start.7) | collective-permute-done | bytes 524320 | tf_op jit(solution)/shard_map/ppermute | solution.py:27
  155.1 2.0 constant_dynamic-update-slice_fusion.15
  157.1 1.9 constant_dynamic-update-slice_fusion.14
  159.0 0.9 constant_dynamic-update-slice_fusion.13
  159.9 0.9 constant_dynamic-update-slice_fusion.12
  161.6 0.9 constant_dynamic-update-slice_fusion.10
  162.5 0.9 constant_dynamic-update-slice_fusion.9
  163.4 0.9 constant_dynamic-update-slice_fusion.8
  164.3 2.0 constant_dynamic-update-slice_fusion.7
  166.2 1.9 constant_dynamic-update-slice_fusion.6
  169.0 0.9 constant_dynamic-update-slice_fusion.4
  169.9 0.9 constant_dynamic-update-slice_fusion.3
  170.8 0.9 constant_dynamic-update-slice_fusion.2
  171.7 0.9 constant_dynamic-update-slice_fusion.1
  172.6 3.1 fusion.20
  175.7 44.0 %all-gather.7.cloned.1.call-done = bf16[2,2048,512]{2,1,0:T(8,128)(2,1)} async-done(((bf16[2,256,512]{2,1,0:T(8,128)(2,1)}), bf16[2,2048,512]{2,1,0:T(8,128)(2,1)}) %all-gather.7.cloned.1.call-update) | async-done | bytes 4194320 | tf_op jit(solution)/shard_map/all_gather | solution.py:22
  219.7 2.5 fusion.19
  222.2 2.4 collective-permute-start
  226.3 3.2 fusion.109
  229.5 5.7 %all-reduce.1 = (f32[320,1]{0,1:T(1,128)S(1)}, f32[320,1]{0,1:T(1,128)S(1)}) all-reduce(f32[320,1]{0,1:T(1,128)S(1)} %broadcast_in_dim.20, f32[320,1]{0,1:T(1,128)S(1)} %broadcast_in_dim.21), channel_id=1, replica_groups=mesh['sp'=8,'tp'=4] {'tp'}, use_global_device_ids=true, to_apply=%region_2.3 | all-reduce | flops 640 | bytes 5120 | tf_op jit(solution)/shard_map/psum | solution.py:51
  235.2 3.7 %convolution_convert_fusion.1 = bf16[320,2048]{1,0:T(8,128)(2,1)} fusion(bf16[2,512,4096]{2,1,0:T(8,128)(2,1)} %constant_dynamic-update-slice_fusion, s32[]{:T(128)S(6)} %select_n.14, f32[320,512]{1,0:T(8,128)S(1)} %get-tuple-element.18, f32[512]{0:T(512)S(1)} %bitcast.182, f32[512]{0:T(512)S(1)} %bitcast.183, f32[320]{0:T(512)S(1)} %get-tuple-element.12, ...), kind=kOutput, calls=%fused_computation.5 | convolution fusion | flops 673218560 | bytes 4069892 | tf_op jit(solution)/shard_map/dot_general | solution.py:61
  239.1 27.9 %reduce-scatter.3.cloned.1.call-done = bf16[320,512]{1,0:T(8,128)(2,1)} async-done(((bf16[320,2048]{1,0:T(8,128)(2,1)}), bf16[320,512]{1,0:T(8,128)(2,1)}) %reduce-scatter.3.cloned.1.call-update) | async-done | bytes 327696 | tf_op jit(solution)/shard_map/reduce_scatter | solution.py:62
  267.0 1.1 fusion.22
  268.1 5.8 %psum.44 = f32[320,1]{0,1:T(1,128)S(1)} all-reduce(f32[320,1]{0,1:T(1,128)S(1)} %broadcast_in_dim.22), channel_id=1, replica_groups=mesh['sp'=8,'tp'=4] {'tp'}, use_global_device_ids=true, to_apply=%region_7.8 | all-reduce | flops 320 | bytes 2560 | tf_op jit(solution)/shard_map/psum | solution.py:64
  273.9 1.9 fusion.25
  275.9 18.9 %all-gather.11.cloned.1.call-done = bf16[320,2048]{1,0:T(8,128)(2,1)} async-done(((bf16[320,512]{1,0:T(8,128)(2,1)}), bf16[320,2048]{1,0:T(8,128)(2,1)}) %all-gather.11.cloned.1.call-update) | async-done | bytes 1310736 | tf_op jit(solution)/shard_map/all_gather | solution.py:32
  294.8 1.7 fusion.3
  296.5 3.1 fusion.21
  300.1 0.9 fusion.18
  301.0 3.4 collective-permute-start.8
  304.4 0.9 fusion.112
  306.1 3.2 fusion.108
  309.3 6.1 %all-reduce = (f32[320,1]{0,1:T(1,128)S(1)}, f32[320,1]{0,1:T(1,128)S(1)}) all-reduce(f32[320,1]{0,1:T(1,128)S(1)} %broadcast_in_dim.23, f32[320,1]{0,1:T(1,128)S(1)} %broadcast_in_dim.24), channel_id=1, replica_groups=mesh['sp'=8,'tp'=4] {'tp'}, use_global_device_ids=true, to_apply=%region_10.11 | all-reduce | flops 640 | bytes 5120 | tf_op jit(solution)/shard_map/psum | solution.py:51
  315.4 3.8 %convolution_convert_fusion = bf16[320,2048]{1,0:T(8,128)(2,1)} fusion(bf16[2,512,4096]{2,1,0:T(8,128)(2,1)} %constant_dynamic-update-slice_fusion, s32[]{:T(128)S(6)} %add.363, s32[]{:T(128)S(6)} %select_n.14, f32[320,512]{1,0:T(8,128)S(1)} %get-tuple-element.17, f32[512]{0:T(512)S(1)} %bitcast.180, f32[512]{0:T(512)S(1)} %bitcast.181, ...), kind=kOutput, calls=%fused_computation.4 | convolution fusion | flops 673218560 | bytes 4069896 | tf_op jit(solution)/shard_map/dot_general | solution.py:61
  319.2 27.4 %reduce-scatter.5.cloned.1.call-done = bf16[320,512]{1,0:T(8,128)(2,1)} async-done(((bf16[320,2048]{1,0:T(8,128)(2,1)}), bf16[320,512]{1,0:T(8,128)(2,1)}) %reduce-scatter.5.cloned.1.call-update) | async-done | bytes 327696 | tf_op jit(solution)/shard_map/reduce_scatter | solution.py:62
  346.6 1.1 fusion.26
  347.7 5.8 %psum.47 = f32[320,1]{0,1:T(1,128)S(1)} all-reduce(f32[320,1]{0,1:T(1,128)S(1)} %broadcast_in_dim.25), channel_id=1, replica_groups=mesh['sp'=8,'tp'=4] {'tp'}, use_global_device_ids=true, to_apply=%region_15.16 | all-reduce | flops 320 | bytes 2560 | tf_op jit(solution)/shard_map/psum | solution.py:64
  353.5 1.9 fusion.29
  (60 shorter events, 10.3 us)
Async XLA Ops:
  6.5 137.2 %all-gather.5.cloned.1.call-start = ((), (), s32[]{:S(2)}) async-start(), calls=%async_computation.2 | async-start | bytes 1638400 | tf_op jit(solution)/shard_map/all_gather | solution.py:32
  7.3 165.4 %all-gather.9.cloned.1.call-start = ((), (), s32[]{:S(2)}) async-start(), calls=%async_computation.4 | async-start | bytes 4718592 | tf_op jit(solution)/shard_map/all_gather | solution.py:23
  8.0 211.7 %all-gather.7.cloned.1.call-start = ((), (), s32[]{:S(2)}) async-start(), calls=%async_computation.3 | async-start | bytes 4718592 | tf_op jit(solution)/shard_map/all_gather | solution.py:22
  8.7 258.3 %reduce-scatter.3.cloned.1.call-start = ((), (), s32[]{:S(2)}) async-start(), calls=%async_computation.5 | async-start | bytes 1638400 | tf_op jit(solution)/shard_map/reduce_scatter | solution.py:62
  8.8 18.2 %collective-permute-start.1 = (bf16[2,512,256]{2,1,0:T(8,128)(2,1)}, bf16[2,512,256]{2,1,0:T(8,128)(2,1)S(1)}, u32[]{:S(2)}, u32[]{:S(2)}) collective-permute-start(bf16[2,512,256]{2,1,0:T(8,128)(2,1)} %param.16), channel_id=1, source_target_pairs={{0,4},{4,8},{8,12},{12,16},{16,20},{20,24},{24,28},{28,0},{1,5},{5... | collective-permute-start | bytes 1572872 | tf_op jit(solution)/shard_map/ppermute | solution.py:27
  27.0 15.8 %collective-permute-start.2 = (bf16[2,512,256]{2,1,0:T(8,128)(2,1)S(1)}, bf16[2,512,256]{2,1,0:T(8,128)(2,1)S(1)}, u32[]{:S(2)}, u32[]{:S(2)}) collective-permute-start(bf16[2,512,256]{2,1,0:T(8,128)(2,1)S(1)} %collective-permute-done.1), channel_id=1, source_target_pairs={{0,4},{4,8},{8,12},{12,16},{16,20},{20,24},{24,28},{28,0},{1,5},{5... | collective-permute-start | bytes 1572872 | tf_op jit(solution)/shard_map/ppermute | solution.py:27
  42.8 27.8 %collective-permute-start.3 = (bf16[2,512,256]{2,1,0:T(8,128)(2,1)S(1)}, bf16[2,512,256]{2,1,0:T(8,128)(2,1)S(1)}, u32[]{:S(2)}, u32[]{:S(2)}) collective-permute-start(bf16[2,512,256]{2,1,0:T(8,128)(2,1)S(1)} %collective-permute-done.2), channel_id=1, source_target_pairs={{0,4},{4,8},{8,12},{12,16},{16,20},{20,24},{24,28},{28,0},{1,5},{5... | collective-permute-start | bytes 1572872 | tf_op jit(solution)/shard_map/ppermute | solution.py:27
  70.6 21.1 %collective-permute-start.4 = (bf16[2,512,256]{2,1,0:T(8,128)(2,1)S(1)}, bf16[2,512,256]{2,1,0:T(8,128)(2,1)S(1)}, u32[]{:S(2)}, u32[]{:S(2)}) collective-permute-start(bf16[2,512,256]{2,1,0:T(8,128)(2,1)S(1)} %collective-permute-done.3), channel_id=1, source_target_pairs={{0,4},{4,8},{8,12},{12,16},{16,20},{20,24},{24,28},{28,0},{1,5},{5... | collective-permute-start | bytes 1572872 | tf_op jit(solution)/shard_map/ppermute | solution.py:27
  91.7 26.9 %collective-permute-start.5 = (bf16[2,512,256]{2,1,0:T(8,128)(2,1)S(1)}, bf16[2,512,256]{2,1,0:T(8,128)(2,1)S(1)}, u32[]{:S(2)}, u32[]{:S(2)}) collective-permute-start(bf16[2,512,256]{2,1,0:T(8,128)(2,1)S(1)} %collective-permute-done.4), channel_id=1, source_target_pairs={{0,4},{4,8},{8,12},{12,16},{16,20},{20,24},{24,28},{28,0},{1,5},{5... | collective-permute-start | bytes 1572872 | tf_op jit(solution)/shard_map/ppermute | solution.py:27
  118.7 24.3 %collective-permute-start.6 = (bf16[2,512,256]{2,1,0:T(8,128)(2,1)S(1)}, bf16[2,512,256]{2,1,0:T(8,128)(2,1)}, u32[]{:S(2)}, u32[]{:S(2)}) collective-permute-start(bf16[2,512,256]{2,1,0:T(8,128)(2,1)S(1)} %collective-permute-done.5), channel_id=1, source_target_pairs={{0,4},{4,8},{8,12},{12,16},{16,20},{20,24},{24,28},{28,0},{1,5},{5... | collective-permute-start | bytes 1572872 | tf_op jit(solution)/shard_map/ppermute | solution.py:27
  142.9 12.2 %collective-permute-start.7 = (bf16[2,512,256]{2,1,0:T(8,128)(2,1)}, bf16[2,512,256]{2,1,0:T(8,128)(2,1)}, u32[]{:S(2)}, u32[]{:S(2)}) collective-permute-start(bf16[2,512,256]{2,1,0:T(8,128)(2,1)} %collective-permute-done.6), channel_id=1, source_target_pairs={{0,4},{4,8},{8,12},{12,16},{16,20},{20,24},{24,28},{28,0},{1,5},{5... | collective-permute-start | bytes 1572872 | tf_op jit(solution)/shard_map/ppermute | solution.py:27
  143.7 19.7 %copy-start.1 = (bf16[2,512,256]{2,1,0:T(8,128)(2,1)S(1)}, bf16[2,512,256]{2,1,0:T(8,128)(2,1)}, u32[]{:S(2)}) copy-start(bf16[2,512,256]{2,1,0:T(8,128)(2,1)} %param.16) | copy-start | bytes 1572868
  172.6 47.1 %copy-start.2 = (bf16[320,2048]{1,0:T(8,128)(2,1)S(1)}, bf16[320,2048]{1,0:T(8,128)(2,1)}, u32[]{:S(2)}) copy-start(bf16[320,2048]{1,0:T(8,128)(2,1)} %all-gather.5.cloned.1.call-done) | copy-start | bytes 3932164
  222.2 4.0 %collective-permute-start = (bf16[30,512]{1,0:T(8,128)(2,1)S(1)}, bf16[30,512]{1,0:T(8,128)(2,1)S(1)}, u32[]{:S(2)}, u32[]{:S(2)}) collective-permute-start(bf16[30,512]{1,0:T(8,128)(2,1)S(1)} %slice.562), channel_id=1, source_target_pairs={{0,4},{4,8},{8,12},{12,16},{16,20},{20,24},{24,28},{1,5},{5,9},{9,... | collective-permute-start | bytes 92168 | tf_op jit(solution)/shard_map/ppermute | solution.py:16
  235.2 3.8 %copy-start.5 = (f32[2,512]{1,0:T(2,128)S(1)}, f32[2,512]{1,0:T(2,128)}, u32[]{:S(2)}) copy-start(f32[2,512]{1,0:T(2,128)} %param.17) | copy-start | bytes 12292
  235.2 38.7 %copy-start.4 = (bf16[320,512]{1,0:T(8,128)(2,1)S(1)}, bf16[320,512]{1,0:T(8,128)(2,1)}, u32[]{:S(2)}) copy-start(bf16[320,512]{1,0:T(8,128)(2,1)} %param.9) | copy-start | bytes 983044
  239.0 55.8 %all-gather.11.cloned.1.call-start = ((), (), s32[]{:S(2)}) async-start(), calls=%async_computation.6 | async-start | bytes 1638400 | tf_op jit(solution)/shard_map/all_gather | solution.py:32
  275.8 70.7 %reduce-scatter.5.cloned.1.call-start = ((), (), s32[]{:S(2)}) async-start(), calls=%async_computation.7 | async-start | bytes 1638400 | tf_op jit(solution)/shard_map/reduce_scatter | solution.py:62
  296.5 3.2 copy-start.3
  296.5 3.6 copy-start.6
  301.0 5.0 %collective-permute-start.8 = (bf16[30,512]{1,0:T(8,128)(2,1)S(1)}, bf16[30,512]{1,0:T(8,128)(2,1)S(1)}, u32[]{:S(2)}, u32[]{:S(2)}) collective-permute-start(bf16[30,512]{1,0:T(8,128)(2,1)S(1)} %slice.596), channel_id=1, source_target_pairs={{0,4},{4,8},{8,12},{12,16},{16,20},{20,24},{24,28},{1,5},{5,9},{9,... | collective-permute-start | bytes 92168 | tf_op jit(solution)/shard_map/ppermute | solution.py:16
  309.2 44.3 %copy-start = (bf16[320,512]{1,0:T(8,128)(2,1)S(1)}, bf16[320,512]{1,0:T(8,128)(2,1)}, u32[]{:S(2)}) copy-start(bf16[320,512]{1,0:T(8,128)(2,1)} %fusion.25) | copy-start | bytes 983044
Sparse Core Ops, SparseCore 0:
  8.9 20.8 all-gather.4
  32.0 101.0 all-gather.8
  135.3 84.3 all-gather.6
  239.1 27.8 reduce-scatter.2
  276.0 18.7 all-gather.10
  319.3 27.2 reduce-scatter.4
